TPU v7x, 32 devices: a whole 2x2x4 slice. The times are simulated.
32 devices in a mesh: fs: 8 (over z, y), tp: 4 (over x, core).
Axes of the slice: x: 2, y: 2, z: 4, core: 2. Of those that a mesh axis runs over, the one named last changes fastest.
Arguments:
- later_gate: bfloat16 [5120, 5632], P('fs', 'tp'), may hold values from -6 to 6
- later_up: bfloat16 [5120, 5632], P('fs', 'tp'), may hold values from -6 to 6
- early_gate: bfloat16 [5120, 5632], P('fs', 'tp'), may hold values from -6 to 6
- early_up: bfloat16 [5120, 5632], P('fs', 'tp'), may hold values from -6 to 6
- early_cotangent: bfloat16 [5120, 2048], P(('fs', 'tp')), may hold values from -6 to 6
- down_weight: bfloat16 [5632, 2048], P('tp', 'fs'), may hold values from -0.078125 to 0.078125
- grad_running: float32 [5632, 2048], P('tp', 'fs'), may hold values from -224 to 224
Outputs:
- mixed: bfloat16 [5120, 2048], P(('fs', 'tp'))
- gate_grad: bfloat16 [5120, 5632], P('fs', 'tp')
- up_grad: bfloat16 [5120, 5632], P('fs', 'tp')
- grad_total: float32 [5632, 2048], P('tp', 'fs')
All inputs are finite; a program needn't handle non-finite values.
Results may differ from a plain program's by a relative error of at most 0.009.
Values may be sent and summed in bfloat16 or wider, within the bound.
A program may use at most 128 MiB of HBM per device.

v0:
```python
import jax
import jax.numpy as jnp
from jax import lax
from jax.sharding import PartitionSpec as P


def on_device(
    later_gate, later_up, early_gate, early_up, early_cotangent, down_weight, grad_running
):
    later_hidden = (
        jax.nn.silu(later_gate.astype(jnp.float32)) * later_up.astype(jnp.float32)
    ).astype(jnp.bfloat16)
    gate_value = early_gate.astype(jnp.float32)
    up_value = early_up.astype(jnp.float32)
    sigma = jax.nn.sigmoid(gate_value)
    early_hidden = (gate_value * sigma * up_value).astype(jnp.bfloat16)
    cot_rows = lax.all_gather(early_cotangent, "tp", axis=0, tiled=True)
    whole = lax.all_gather(down_weight, "fs", axis=1, tiled=True)
    mixed = lax.psum_scatter(
        jnp.dot(later_hidden, whole, preferred_element_type=jnp.float32).astype(jnp.bfloat16),
        "tp",
        scatter_dimension=0,
        tiled=True,
    )
    hidden_cot = lax.dot_general(
        cot_rows, whole, (((1,), (1,)), ((), ())), preferred_element_type=jnp.float32
    )
    gate_grad = (hidden_cot * up_value * sigma * (1.0 + gate_value * (1.0 - sigma))).astype(
        jnp.bfloat16
    )
    up_grad = (hidden_cot * gate_value * sigma).astype(jnp.bfloat16)
    summed = lax.psum_scatter(
        lax.dot_general(
            cot_rows, early_hidden, (((0,), (0,)), ((), ())), preferred_element_type=jnp.float32
        ),
        "fs",
        scatter_dimension=0,
        tiled=True,
    )
    grad_total = grad_running + summed.T
    return (mixed, gate_grad, up_grad, grad_total)


def solution(mesh):
    placed = (
        P("fs", "tp"),
        P("fs", "tp"),
        P("fs", "tp"),
        P("fs", "tp"),
        P(("fs", "tp"), None),
        P("tp", "fs"),
        P("tp", "fs"),
    )
    return jax.shard_map(
        on_device,
        mesh=mesh,
        in_specs=placed,
        out_specs=(P(("fs", "tp"), None), P("fs", "tp"), P("fs", "tp"), P("tp", "fs")),
        check_vma=False,
    )
```

profile of v0, /device:TPU:0, one launch (start us, length us, event | category | flops | bytes accessed | tf_op | source)
XLA Modules:
  0.0 371.2 jit_solution(2300562633143723769)
XLA Ops:
  7.2 0.0 all-gather.5.cloned.1.call-start
  7.2 0.7 all-gather.5.cloned.1.call-update
  7.9 0.0 all-gather.3.cloned.1.call-start
  7.9 0.7 all-gather.3.cloned.1.call-update
  8.6 0.0 reduce-scatter.5.cloned.1.call-start
  8.7 29.1 %all-gather.5.cloned.1.call-done = bf16[640,2048]{1,0:T(8,128)(2,1)} async-done(((bf16[160,2048]{1,0:T(8,128)(2,1)}), bf16[640,2048]{1,0:T(8,128)(2,1)}) %all-gather.5.cloned.1.call-update) | async-done | bytes 2621456 | tf_op jit(solution)/shard_map/all_gather | solution.py:17
  37.8 12.2 %convolution_bitcast_fusion = f32[2048,1408]{0,1:T(8,128)} fusion(bf16[640,2048]{1,0:T(8,128)(2,1)} %all-gather.5.cloned.1.call-done, bf16[640,1408]{1,0:T(8,128)(2,1)} %param.10, bf16[640,1408]{1,0:T(8,128)(2,1)} %param.9), kind=kOutput, calls=%fused_computation | convolution fusion | flops 3698196480 | bytes 17760256 | tf_op jit(solution)/shard_map/dot_general | solution.py:33
  50.0 0.0 copy-start.1
  50.0 0.0 reduce-scatter.5.cloned.1.call-update
  50.1 0.2 reduce-scatter.3.cloned.1.call-start
  50.3 82.7 %all-gather.3.cloned.1.call-done = bf16[1408,2048]{1,0:T(8,128)(2,1)} async-done(((bf16[1408,256]{1,0:T(8,128)(2,1)}), bf16[1408,2048]{1,0:T(8,128)(2,1)}) %all-gather.3.cloned.1.call-update) | async-done | bytes 5767184 | tf_op jit(solution)/shard_map/all_gather | solution.py:18
  133.0 0.0 copy-done.1
  133.0 9.2 %convolution_convert_fusion = bf16[640,2048]{1,0:T(8,128)(2,1)} fusion(bf16[1408,2048]{1,0:T(8,128)(2,1)} %all-gather.3.cloned.1.call-done, bf16[640,1408]{1,0:T(8,128)(2,1)S(1)} %copy-done.1, bf16[640,1408]{1,0:T(8,128)(2,1)} %param.7), kind=kOutput, calls=%fused_computation.24 | convolution fusion | flops 3699507200 | bytes 11993088 | tf_op jit(solution)/shard_map/dot_general | solution.py:20
  142.2 0.0 reduce-scatter.3.cloned.1.call-update
  142.2 0.0 copy-start
  142.3 12.0 %fusion.13 = (bf16[640,1408]{1,0:T(8,128)(2,1)}, bf16[640,1408]{1,0:T(8,128)(2,1)}) fusion(bf16[640,1408]{1,0:T(8,128)(2,1)} %param.9, bf16[640,1408]{1,0:T(8,128)(2,1)} %param.10, bf16[640,2048]{1,0:T(8,128)(2,1)} %all-gather.5.cloned.1.call-done, bf16[1408,2048]{1,0:T(8,128)(2,1)} %all-gather.3.cloned.1.call-done), kind=kOutput, calls=%fused_computation.22 | convolution fusion | flops 3704504320 | bytes 15597568 | tf_op jit(solution)/shard_map/dot_general | solution.py:25
  154.3 173.8 %reduce-scatter.5.cloned.1.call-done = f32[256,1408]{0,1:T(8,128)} async-done(((f32[2048,1408]{0,1:T(8,128)}), f32[256,1408]{0,1:T(8,128)}) %reduce-scatter.5.cloned.1.call-update) | async-done | bytes 1441808 | tf_op jit(solution)/shard_map/reduce_scatter | solution.py:32
  328.1 0.0 copy-done
  328.1 2.6 bitcast_add_fusion
  330.7 33.9 %reduce-scatter.3.cloned.1.call-done = bf16[160,2048]{1,0:T(8,128)(2,1)} async-done(((bf16[640,2048]{1,0:T(8,128)(2,1)}), bf16[160,2048]{1,0:T(8,128)(2,1)}) %reduce-scatter.3.cloned.1.call-update) | async-done | bytes 655376 | tf_op jit(solution)/shard_map/reduce_scatter | solution.py:19
Async XLA Ops:
  7.2 30.7 %all-gather.5.cloned.1.call-start = ((), (), s32[]{:S(2)}) async-start(), calls=%async_computation.4 | async-start | bytes 3276800 | tf_op jit(solution)/shard_map/all_gather | solution.py:17
  7.9 125.1 %all-gather.3.cloned.1.call-start = ((), (), s32[]{:S(2)}) async-start(), calls=%async_computation.2 | async-start | bytes 6488064 | tf_op jit(solution)/shard_map/all_gather | solution.py:18
  8.6 319.4 %reduce-scatter.5.cloned.1.call-start = ((), (), s32[]{:S(2)}) async-start(), calls=%async_computation.5 | async-start | bytes 12976128 | tf_op jit(solution)/shard_map/reduce_scatter | solution.py:32
  50.0 83.0 %copy-start.1 = (bf16[640,1408]{1,0:T(8,128)(2,1)S(1)}, bf16[640,1408]{1,0:T(8,128)(2,1)}, u32[]{:S(2)}) copy-start(bf16[640,1408]{1,0:T(8,128)(2,1)} %param.8) | copy-start | bytes 5406724
  50.1 314.6 %reduce-scatter.3.cloned.1.call-start = ((), (), s32[]{:S(2)}) async-start(), calls=%async_computation.3 | async-start | bytes 3276800 | tf_op jit(solution)/shard_map/reduce_scatter | solution.py:19
  142.2 185.8 %copy-start = (f32[1408,256]{1,0:T(8,128)S(1)}, f32[1408,256]{1,0:T(8,128)}, u32[]{:S(2)}) copy-start(f32[1408,256]{1,0:T(8,128)} %param.13) | copy-start | bytes 4325380
Sparse Core Ops, SparseCore 0:
  9.5 28.2 all-gather.4
  39.9 93.1 all-gather.2
  136.6 191.4 reduce-scatter.4
  331.1 33.5 reduce-scatter.2
where the time goes:
time: 371 us
  waiting for transfers between devices  321 us (87%)
  matrix products  33.4 us (9%)
  between operations  13.8 us (4%)
    reduce_scatter x1, waiting for transfers between devices, on_device(): lax.psum_scatter(lax.dot_general(cot_rows, early_hidden, (((0,), (0,)), (...  174 us
    all_gather x1, waiting for transfers between devices, on_device(): whole = lax.all_gather(down_weight, 'fs', axis=1, tiled=True)  82.7 us
    reduce_scatter x1, waiting for transfers between devices, on_device(): lax.psum_scatter(jnp.dot(later_hidden, whole, preferred_element_type=jnp....  33.9 us
    all_gather x1, waiting for transfers between devices, on_device(): cot_rows = lax.all_gather(early_cotangent, 'tp', axis=0, tiled=True)  29.1 us
    dot_general x1, matrix products, on_device(): lax.dot_general(cot_rows, early_hidden, (((0,), (0,)), ((), ())), preferr...  12.2 us
    dot_general x1, matrix products, on_device(): lax.dot_general(cot_rows, whole, (((1,), (1,)), ((), ())), preferred_elem...  12 us
    dot_general x1, matrix products, on_device(): jnp.dot(later_hidden, whole, preferred_element_type=jnp.float32)  9.19 us
  transfers between devices with their start and end apart: 4, of which 4 were waited for; matrix products, arithmetic and copies ran while one was open for 10% of the time, Pallas kernels for 0%

commit v1 on v0

--- a/solution.py
+++ b/solution.py
@@ -15,7 +15,12 @@
     sigma = jax.nn.sigmoid(gate_value)
     early_hidden = (gate_value * sigma * up_value).astype(jnp.bfloat16)
     cot_rows = lax.all_gather(early_cotangent, "tp", axis=0, tiled=True)
-    whole = lax.all_gather(down_weight, "fs", axis=1, tiled=True)
+    ring = [down_weight]
+    for hop in range(7):
+        ring.append(lax.ppermute(ring[-1], "fs", [(dev, (dev + 1) % 8) for dev in range(8)]))
+    whole = jnp.roll(
+        jnp.concatenate(ring[::-1], axis=1), (lax.axis_index("fs") + 1) * ring[0].shape[1], axis=1
+    )
     mixed = lax.psum_scatter(
         jnp.dot(later_hidden, whole, preferred_element_type=jnp.float32).astype(jnp.bfloat16),
         "tp",

time: 371 us -> 393 us (1.059)
  local copies, waits for them, and re-layouts: 0.01 us -> 34.2 us
  waiting for transfers between devices: 321 us -> 310 us
    ppermute x0 -> x7, waiting for transfers between devices: none -> 212 us  [on_device(): lax.ppermute(ring[-1], 'fs', [(dev, (dev + 1) % 8) for dev in range(8)])]
    reduce_scatter x1, waiting for transfers between devices: 174 us -> 39.4 us  [on_device(): lax.psum_scatter(lax.dot_general(cot_rows, early_hidden, (((0,), (0,)), (...]
    all_gather x1 -> x0, waiting for transfers between devices: 82.7 us -> none  [on_device(): whole = lax.all_gather(down_weight, 'fs', axis=1, tiled=True)]
    unnamed x4 -> x43, local copies, waits for them, and re-layouts: 0.01 us -> 34.1 us
    all_gather x1, waiting for transfers between devices: 29.1 us -> 23.8 us  [on_device(): cot_rows = lax.all_gather(early_cotangent, 'tp', axis=0, tiled=True)]
  transfers between devices with their start and end apart: 4 -> 10, of which waited for: 4 -> 10; matrix products, arithmetic and copies ran while one was open for 10% -> 12% of each run, Pallas kernels for 0% -> 0%
where the time goes in v1:
time: 393 us; the launch traced here: 392 us
  waiting for transfers between devices  310 us (79%)
  local copies, waits for them, and re-layouts  34.2 us (9%)
  matrix products  29.7 us (8%)
  between operations  14 us (4%)
    ppermute x7, waiting for transfers between devices, on_device(): lax.ppermute(ring[-1], 'fs', [(dev, (dev + 1) % 8) for dev in range(8)])  212 us
    reduce_scatter x1, waiting for transfers between devices, on_device(): lax.psum_scatter(lax.dot_general(cot_rows, early_hidden, (((0,), (0,)), (...  39.4 us
    unnamed x43, local copies, waits for them, and re-layouts  34.1 us
    reduce_scatter x1, waiting for transfers between devices, on_device(): lax.psum_scatter(jnp.dot(later_hidden, whole, preferred_element_type=jnp....  33.7 us
    all_gather x1, waiting for transfers between devices, on_device(): cot_rows = lax.all_gather(early_cotangent, 'tp', axis=0, tiled=True)  23.8 us
    dot_general x1, matrix products, on_device(): lax.dot_general(cot_rows, early_hidden, (((0,), (0,)), ((), ())), preferr...  12 us
    dot_general x1, matrix products, on_device(): lax.dot_general(cot_rows, whole, (((1,), (1,)), ((), ())), preferred_elem...  11.6 us
  transfers between devices with their start and end apart: 10, of which 10 were waited for; matrix products, arithmetic and copies ran while one was open for 12% of the time, Pallas kernels for 0%

profile of v1, /device:TPU:0, one launch (start us, length us, event | category | flops | bytes accessed | tf_op | source)
XLA Modules:
  0.0 392.2 jit_solution(6852850012753060098)
XLA Ops:
  7.2 0.0 all-gather.2.cloned.1.call-start
  7.2 0.7 all-gather.2.cloned.1.call-update
  7.9 0.0 reduce-scatter.5.cloned.1.call-start
  8.0 3.8 copy.13
  11.7 2.3 copy.14
  14.0 23.8 %all-gather.2.cloned.1.call-done = bf16[640,2048]{1,0:T(8,128)(2,1)} async-done(((bf16[160,2048]{1,0:T(8,128)(2,1)}), bf16[640,2048]{1,0:T(8,128)(2,1)}) %all-gather.2.cloned.1.call-update) | async-done | bytes 2621456 | tf_op jit(solution)/shard_map/all_gather | solution.py:17
  37.8 12.0 %convolution_bitcast_fusion = f32[2048,1408]{0,1:T(8,128)} fusion(bf16[640,2048]{1,0:T(8,128)(2,1)} %all-gather.2.cloned.1.call-done, bf16[640,1408]{0,1:T(8,128)(2,1)} %copy.13, bf16[640,1408]{0,1:T(8,128)(2,1)} %copy.14), kind=kOutput, calls=%fused_computation | convolution fusion | flops 3698196480 | bytes 17760256 | tf_op jit(solution)/shard_map/dot_general | solution.py:38
  49.8 0.0 reduce-scatter.5.cloned.1.call-update
  49.8 0.0 reduce-scatter.3.cloned.1.call-start
  49.9 1.0 copy-done
  50.9 1.5 collective-permute-start
  52.4 30.3 %collective-permute-done = bf16[1408,256]{1,0:T(8,128)(2,1)S(1)} collective-permute-done((bf16[1408,256]{1,0:T(8,128)(2,1)S(1)}, bf16[1408,256]{1,0:T(8,128)(2,1)S(1)}, u32[]{:S(2)}, u32[]{:S(2)}) %collective-permute-start) | collective-permute-done | bytes 720928 | tf_op jit(solution)/shard_map/ppermute | solution.py:20
  82.7 36.2 %collective-permute-done.1 = bf16[1408,256]{1,0:T(8,128)(2,1)S(1)} collective-permute-done((bf16[1408,256]{1,0:T(8,128)(2,1)S(1)}, bf16[1408,256]{1,0:T(8,128)(2,1)S(1)}, u32[]{:S(2)}, u32[]{:S(2)}) %collective-permute-start.1) | collective-permute-done | bytes 720928 | tf_op jit(solution)/shard_map/ppermute | solution.py:20
  118.8 39.0 %collective-permute-done.2 = bf16[1408,256]{1,0:T(8,128)(2,1)S(1)} collective-permute-done((bf16[1408,256]{1,0:T(8,128)(2,1)S(1)}, bf16[1408,256]{1,0:T(8,128)(2,1)S(1)}, u32[]{:S(2)}, u32[]{:S(2)}) %collective-permute-start.2) | collective-permute-done | bytes 720928 | tf_op jit(solution)/shard_map/ppermute | solution.py:20
  157.8 34.4 %collective-permute-done.3 = bf16[1408,256]{1,0:T(8,128)(2,1)S(1)} collective-permute-done((bf16[1408,256]{1,0:T(8,128)(2,1)S(1)}, bf16[1408,256]{1,0:T(8,128)(2,1)S(1)}, u32[]{:S(2)}, u32[]{:S(2)}) %collective-permute-start.3) | collective-permute-done | bytes 720928 | tf_op jit(solution)/shard_map/ppermute | solution.py:20
  192.2 0.9 copy-done.1
  193.1 33.5 %collective-permute-done.4 = bf16[1408,256]{1,0:T(8,128)(2,1)S(1)} collective-permute-done((bf16[1408,256]{1,0:T(8,128)(2,1)S(1)}, bf16[1408,256]{1,0:T(8,128)(2,1)S(1)}, u32[]{:S(2)}, u32[]{:S(2)}) %collective-permute-start.4) | collective-permute-done | bytes 720928 | tf_op jit(solution)/shard_map/ppermute | solution.py:20
  226.6 0.9 copy-done.3
  227.5 20.4 %collective-permute-done.5 = bf16[1408,256]{1,0:T(8,128)(2,1)} collective-permute-done((bf16[1408,256]{1,0:T(8,128)(2,1)S(1)}, bf16[1408,256]{1,0:T(8,128)(2,1)}, u32[]{:S(2)}, u32[]{:S(2)}) %collective-permute-start.5) | collective-permute-done | bytes 720928 | tf_op jit(solution)/shard_map/ppermute | solution.py:20
  247.9 3.8 copy.11
  251.6 3.8 copy.12
  255.5 18.3 %collective-permute-done.6 = bf16[1408,256]{1,0:T(8,128)(2,1)} collective-permute-done((bf16[1408,256]{1,0:T(8,128)(2,1)}, bf16[1408,256]{1,0:T(8,128)(2,1)}, u32[]{:S(2)}, u32[]{:S(2)}) %collective-permute-start.6) | collective-permute-done | bytes 720928 | tf_op jit(solution)/shard_map/ppermute | solution.py:20
  273.8 1.2 constant_dynamic-update-slice_fusion.15
  275.0 1.2 constant_dynamic-update-slice_fusion.14
  276.2 1.2 constant_dynamic-update-slice_fusion.13
  277.4 0.1 constant_dynamic-update-slice_fusion.12
  277.5 0.1 constant_dynamic-update-slice_fusion.11
  277.6 0.0 copy-start.4
  277.6 0.1 constant_dynamic-update-slice_fusion.10
  277.7 0.1 constant_dynamic-update-slice_fusion.9
  277.8 0.1 constant_dynamic-update-slice_fusion.8
  277.9 1.2 constant_dynamic-update-slice_fusion.7
  279.2 1.2 constant_dynamic-update-slice_fusion.6
  280.4 0.1 constant_dynamic-update-slice_fusion.5
  280.5 0.1 constant_dynamic-update-slice_fusion.4
  280.6 0.1 constant_dynamic-update-slice_fusion.3
  280.7 0.1 constant_dynamic-update-slice_fusion.2
  280.8 0.1 constant_dynamic-update-slice_fusion.1
  280.9 0.1 constant_dynamic-update-slice_fusion
  281.0 4.5 %copy-done.10 = bf16[1408,4096]{1,0:T(8,128)(2,1)} copy-done((bf16[1408,4096]{1,0:T(8,128)(2,1)}, bf16[1408,4096]{1,0:T(8,128)(2,1)S(1)}, u32[]{:S(2)}) %copy-start.10) | copy-done | bytes 11534360
  285.6 6.1 %fusion.19 = bf16[640,2048]{1,0:T(8,128)(2,1)} fusion(bf16[1408,4096]{1,0:T(8,128)(2,1)S(1)} %constant_dynamic-update-slice_fusion, s32[]{:T(128)S(6)} %select_n.14, bf16[640,1408]{0,1:T(8,128)(2,1)S(1)} %copy-done.8, bf16[640,1408]{0,1:T(8,128)(2,1)S(1)} %copy-done.7), kind=kOutput, calls=%fused_computation.28 | convolution fusion | flops 3699507200 | bytes 11993092 | tf_op jit(solution)/shard_map/dot_general | solution.py:25
  291.7 0.0 reduce-scatter.3.cloned.1.call-update
  291.7 11.6 %fusion.17 = (bf16[640,1408]{0,1:T(8,128)(2,1)}, bf16[640,1408]{0,1:T(8,128)(2,1)}) fusion(bf16[640,1408]{0,1:T(8,128)(2,1)} %copy.14, bf16[640,1408]{0,1:T(8,128)(2,1)S(1)} %copy-done.6, bf16[640,2048]{1,0:T(8,128)(2,1)} %all-gather.2.cloned.1.call-done, bf16[1408,4096]{1,0:T(8,128)(2,1)} %copy-done.10, s32[]{:T(128)S(6)} %select_n.14), kind=kOutput, calls=%fused_computation.26 | convolution fusion | flops 3704504320 | bytes 15597572 | tf_op jit(solution)/shard_map/dot_general | solution.py:30
  303.3 3.9 copy.15
  307.2 2.3 copy.16
  309.5 39.4 %reduce-scatter.5.cloned.1.call-done = f32[256,1408]{0,1:T(8,128)} async-done(((f32[2048,1408]{0,1:T(8,128)}), f32[256,1408]{0,1:T(8,128)}) %reduce-scatter.5.cloned.1.call-update) | async-done | bytes 1441808 | tf_op jit(solution)/shard_map/reduce_scatter | solution.py:37
  348.9 3.1 bitcast_add_fusion
  352.0 33.7 %reduce-scatter.3.cloned.1.call-done = bf16[160,2048]{1,0:T(8,128)(2,1)} async-done(((bf16[640,2048]{1,0:T(8,128)(2,1)}), bf16[160,2048]{1,0:T(8,128)(2,1)}) %reduce-scatter.3.cloned.1.call-update) | async-done | bytes 655376 | tf_op jit(solution)/shard_map/reduce_scatter | solution.py:24
  (23 shorter events, 0.1 us)
Async XLA Ops:
  7.2 4.6 %copy-start.5 = (bf16[640,1408]{1,0:T(8,128)(2,1)S(1)}, bf16[640,1408]{1,0:T(8,128)(2,1)}, u32[]{:S(2)}) copy-start(bf16[640,1408]{1,0:T(8,128)(2,1)} %param.9) | copy-start | bytes 5406724
  7.2 30.7 %all-gather.2.cloned.1.call-start = ((), (), s32[]{:S(2)}) async-start(), calls=%async_computation.3 | async-start | bytes 3276800 | tf_op jit(solution)/shard_map/all_gather | solution.py:17
  7.9 341.0 %reduce-scatter.5.cloned.1.call-start = ((), (), s32[]{:S(2)}) async-start(), calls=%async_computation.4 | async-start | bytes 12976128 | tf_op jit(solution)/shard_map/reduce_scatter | solution.py:37
  49.8 1.1 copy-start
  49.8 335.8 %reduce-scatter.3.cloned.1.call-start = ((), (), s32[]{:S(2)}) async-start(), calls=%async_computation.2 | async-start | bytes 3276800 | tf_op jit(solution)/shard_map/reduce_scatter | solution.py:24
  50.9 31.7 %collective-permute-start = (bf16[1408,256]{1,0:T(8,128)(2,1)S(1)}, bf16[1408,256]{1,0:T(8,128)(2,1)S(1)}, u32[]{:S(2)}, u32[]{:S(2)}) collective-permute-start(bf16[1408,256]{1,0:T(8,128)(2,1)S(1)} %copy-done), channel_id=1, source_target_pairs={{0,4},{4,8},{8,12},{12,16},{16,20},{20,24},{24,28},{28,0},{1,5},{5... | collective-permute-start | bytes 2162696 | tf_op jit(solution)/shard_map/ppermute | solution.py:20
  82.7 36.2 %collective-permute-start.1 = (bf16[1408,256]{1,0:T(8,128)(2,1)S(1)}, bf16[1408,256]{1,0:T(8,128)(2,1)S(1)}, u32[]{:S(2)}, u32[]{:S(2)}) collective-permute-start(bf16[1408,256]{1,0:T(8,128)(2,1)S(1)} %collective-permute-done), channel_id=1, source_target_pairs={{0,4},{4,8},{8,12},{12,16},{16,20},{20,24},{24,28},{28,0},{1,5},{5... | collective-permute-start | bytes 2162696 | tf_op jit(solution)/shard_map/ppermute | solution.py:20
  118.8 39.0 %collective-permute-start.2 = (bf16[1408,256]{1,0:T(8,128)(2,1)S(1)}, bf16[1408,256]{1,0:T(8,128)(2,1)S(1)}, u32[]{:S(2)}, u32[]{:S(2)}) collective-permute-start(bf16[1408,256]{1,0:T(8,128)(2,1)S(1)} %collective-permute-done.1), channel_id=1, source_target_pairs={{0,4},{4,8},{8,12},{12,16},{16,20},{20,24},{24,28},{28,0},{1,5},{5... | collective-permute-start | bytes 2162696 | tf_op jit(solution)/shard_map/ppermute | solution.py:20
  157.8 34.4 %collective-permute-start.3 = (bf16[1408,256]{1,0:T(8,128)(2,1)S(1)}, bf16[1408,256]{1,0:T(8,128)(2,1)S(1)}, u32[]{:S(2)}, u32[]{:S(2)}) collective-permute-start(bf16[1408,256]{1,0:T(8,128)(2,1)S(1)} %collective-permute-done.2), channel_id=1, source_target_pairs={{0,4},{4,8},{8,12},{12,16},{16,20},{20,24},{24,28},{28,0},{1,5},{5... | collective-permute-start | bytes 2162696 | tf_op jit(solution)/shard_map/ppermute | solution.py:20
  192.2 0.9 copy-start.1
  193.1 33.5 %collective-permute-start.4 = (bf16[1408,256]{1,0:T(8,128)(2,1)S(1)}, bf16[1408,256]{1,0:T(8,128)(2,1)S(1)}, u32[]{:S(2)}, u32[]{:S(2)}) collective-permute-start(bf16[1408,256]{1,0:T(8,128)(2,1)S(1)} %collective-permute-done.3), channel_id=1, source_target_pairs={{0,4},{4,8},{8,12},{12,16},{16,20},{20,24},{24,28},{28,0},{1,5},{5... | collective-permute-start | bytes 2162696 | tf_op jit(solution)/shard_map/ppermute | solution.py:20
  226.6 0.9 copy-start.3
  227.5 20.4 %collective-permute-start.5 = (bf16[1408,256]{1,0:T(8,128)(2,1)S(1)}, bf16[1408,256]{1,0:T(8,128)(2,1)}, u32[]{:S(2)}, u32[]{:S(2)}) collective-permute-start(bf16[1408,256]{1,0:T(8,128)(2,1)S(1)} %collective-permute-done.4), channel_id=1, source_target_pairs={{0,4},{4,8},{8,12},{12,16},{16,20},{20,24},{24,28},{28,0},{1,5},{5... | collective-permute-start | bytes 2162696 | tf_op jit(solution)/shard_map/ppermute | solution.py:20
  247.9 25.9 %collective-permute-start.6 = (bf16[1408,256]{1,0:T(8,128)(2,1)}, bf16[1408,256]{1,0:T(8,128)(2,1)}, u32[]{:S(2)}, u32[]{:S(2)}) collective-permute-start(bf16[1408,256]{1,0:T(8,128)(2,1)} %collective-permute-done.5), channel_id=1, source_target_pairs={{0,4},{4,8},{8,12},{12,16},{16,20},{20,24},{24,28},{28,0},{1,5},{5... | collective-permute-start | bytes 2162696 | tf_op jit(solution)/shard_map/ppermute | solution.py:20
  255.5 22.0 %copy-start.2 = (bf16[1408,256]{1,0:T(8,128)(2,1)S(1)}, bf16[1408,256]{1,0:T(8,128)(2,1)}, u32[]{:S(2)}) copy-start(bf16[1408,256]{1,0:T(8,128)(2,1)} %copy-done.1) | copy-start | bytes 2162692
  277.6 2.7 copy-start.4
  280.5 5.1 %copy-start.7 = (bf16[640,1408]{0,1:T(8,128)(2,1)S(1)}, bf16[640,1408]{0,1:T(8,128)(2,1)}, u32[]{:S(2)}) copy-start(bf16[640,1408]{0,1:T(8,128)(2,1)} %copy.11) | copy-start | bytes 5406724
  280.5 5.1 %copy-start.8 = (bf16[640,1408]{0,1:T(8,128)(2,1)S(1)}, bf16[640,1408]{0,1:T(8,128)(2,1)}, u32[]{:S(2)}) copy-start(bf16[640,1408]{0,1:T(8,128)(2,1)} %copy.12) | copy-start | bytes 5406724
  281.0 4.5 %copy-start.10 = (bf16[1408,4096]{1,0:T(8,128)(2,1)}, bf16[1408,4096]{1,0:T(8,128)(2,1)S(1)}, u32[]{:S(2)}) copy-start(bf16[1408,4096]{1,0:T(8,128)(2,1)S(1)} %constant_dynamic-update-slice_fusion) | copy-start | bytes 34603012
  285.6 6.2 %copy-start.6 = (bf16[640,1408]{0,1:T(8,128)(2,1)S(1)}, bf16[640,1408]{0,1:T(8,128)(2,1)}, u32[]{:S(2)}) copy-start(bf16[640,1408]{0,1:T(8,128)(2,1)} %copy.13) | copy-start | bytes 5406724
  303.3 3.9 copy-start.9
Sparse Core Ops, SparseCore 0:
  9.5 28.2 all-gather.1
  50.0 298.8 reduce-scatter.4
  352.0 33.5 reduce-scatter.2
